TPU v7x, 128 devices: a whole 4x4x4 slice. The times are simulated.
128 devices in a mesh: ep: 128 (over z, y, x, core).
Axes of the slice: x: 4, y: 4, z: 4, core: 2. Of those that a mesh axis runs over, the one named last changes fastest.
Arguments:
- hidden: bfloat16 [4096, 2048], P('ep'), may hold values from -6 to 6
- cache_keys: bfloat16 [4096, 1024, 128], P('ep'), may hold values from -512 to 512
- cache_values: bfloat16 [4096, 1024, 128], P('ep'), may hold values from -6 to 6
- lengths: int32 [4096], P('ep'), may hold values from 1 to 1024
- first_gain: float32 [2048], replicated, may hold values from 0.1 to 1.9
- query_weight: bfloat16 [2048, 1024], replicated, may hold values from -0.125 to 0.125
- key_weight: bfloat16 [2048, 128], replicated, may hold values from -0.125 to 0.125
- value_weight: bfloat16 [2048, 128], replicated, may hold values from -0.125 to 0.125
- mixing: float32 [8], replicated, may hold values from 0.3 to 0.8
- head_gain: float32 [128], replicated, may hold values from 0.1 to 1.9
- out_weight: bfloat16 [1024, 2048], replicated, may hold values from -0.1875 to 0.1875
- second_gain: float32 [2048], replicated, may hold values from 0.1 to 1.9
- routes: int32 [4096, 4], P('ep'), may hold values from 0 to 63, as said below
- route_weight: float32 [4096, 4], P('ep'), may hold values from 0.05 to 1
- expert_gate: bfloat16 [128, 2048, 256], P('ep'), may hold values from -0.125 to 0.125
- expert_up: bfloat16 [128, 2048, 256], P('ep'), may hold values from -0.125 to 0.125
- expert_down: bfloat16 [128, 256, 2048], P('ep'), may hold values from -0.25 to 0.25
Outputs:
- layer_out: bfloat16 [4096, 2048], P('ep')
- new_key: bfloat16 [4096, 128], P('ep')
- new_value: bfloat16 [4096, 128], P('ep')
Inputs may be any that keep to these rules, and one draw needn't show every extreme that they name: `routes`: each row names 4 different experts of one group, that is of one block of 16 consecutive numbers. Among the rows of one device, two rows name the same set of experts or disjoint sets, and no expert is named by more than 4 rows; one and the same expert is named by exactly 4 rows on every device.
All inputs are finite; a program needn't handle non-finite values.
Results may differ from a plain program's by a relative error of at most 0.025.
Values may be sent and summed in bfloat16 or wider, within the bound.
No kernel may reach another device: no remote copies, remote signals or barrier semaphores. Data moves between devices by JAX's collectives and lax.ppermute only.
A program may use at most 128 MiB of HBM per device.

v0:
```python
import jax
import jax.numpy as jnp
from jax import lax
from jax.sharding import PartitionSpec as P

D = 2048
HEADS = 8
DK = 64
DV = 128
EXP_SPLIT = 2
TOP_K = 4


epsilon = 1e-06


def root_scale(rows, gain):
    values = rows.astype(jnp.float32)
    factor = lax.rsqrt(jnp.mean(values * values, axis=-1, keepdims=True) + epsilon)
    return values * factor * gain


def slot_tables(routes, experts, capacity):
    count, picks = routes.shape
    flat = routes.reshape(count * picks)
    indicator = (flat[:, None] == jnp.arange(experts, dtype=jnp.int32)[None, :]).astype(jnp.int32)
    before = jnp.cumsum(indicator, axis=0) - indicator
    place = jnp.sum(before * indicator, axis=1)
    target = flat * capacity + place
    slots = jnp.arange(experts * capacity, dtype=jnp.int32)
    match = target[None, :] == slots[:, None]
    return match.reshape(experts * capacity, count, picks)


def attend(query, new_key, new_value, cache_keys, cache_values, lengths, mixing):
    count = query.shape[0]
    span = cache_keys.shape[1]
    queries = query.reshape(count, HEADS, 2, DK)
    keys = cache_keys.reshape(count, span, 2, DK)
    scores = jnp.einsum(
        "shmd,slmd->shml", queries, keys, preferred_element_type=jnp.float32
    ) * DK ** (-0.5)
    own_scores = jnp.einsum(
        "shmd,smd->shm", queries, new_key.reshape(count, 2, DK), preferred_element_type=jnp.float32
    ) * DK ** (-0.5)
    valid = jnp.arange(span, dtype=jnp.int32)[None, :] < lengths[:, None]
    scores = jnp.where(valid[:, None, None, :], scores, -jnp.inf)
    highest = jnp.maximum(jnp.max(scores, axis=-1), own_scores)
    weights = jnp.exp(scores - highest[..., None])
    own_weights = jnp.exp(own_scores - highest)
    total = jnp.sum(weights, axis=-1) + own_weights
    weights = weights / total[..., None]
    own_weights = own_weights / total
    contrast = (weights[:, :, 0] - mixing[None, :, None] * weights[:, :, 1]).astype(jnp.bfloat16)
    own_contrast = (own_weights[:, :, 0] - mixing[None, :] * own_weights[:, :, 1]).astype(
        jnp.bfloat16
    )
    mixed = jnp.einsum("shl,sle->she", contrast, cache_values, preferred_element_type=jnp.float32)
    return (
        mixed
        + own_contrast.astype(jnp.float32)[..., None] * new_value.astype(jnp.float32)[:, None, :]
    )


def head_norm(mixed, head_gain):
    factor = lax.rsqrt(jnp.mean(mixed * mixed, axis=-1, keepdims=True) + epsilon)
    scaled = mixed * factor * head_gain
    return scaled.reshape(mixed.shape[0], HEADS * DV).astype(jnp.bfloat16)


def expert_apply(flat, expert_gate, expert_up, expert_down):
    gate = jnp.dot(flat, expert_gate[0], preferred_element_type=jnp.float32)
    upper = jnp.dot(flat, expert_up[0], preferred_element_type=jnp.float32)
    inner = (jax.nn.silu(gate) * upper).astype(jnp.bfloat16)
    return jnp.dot(inner, expert_down[0], preferred_element_type=jnp.float32).astype(jnp.bfloat16)


def per_device(
    hidden,
    cache_keys,
    cache_values,
    lengths,
    first_gain,
    query_weight,
    key_weight,
    value_weight,
    mixing,
    head_gain,
    out_weight,
    second_gain,
    routes,
    route_weight,
    expert_gate,
    expert_up,
    expert_down,
):
    count = hidden.shape[0]
    normed = root_scale(hidden, first_gain).astype(jnp.bfloat16)
    query = jnp.dot(normed, query_weight, preferred_element_type=jnp.float32).astype(jnp.bfloat16)
    new_key = jnp.dot(normed, key_weight, preferred_element_type=jnp.float32).astype(jnp.bfloat16)
    new_value = jnp.dot(normed, value_weight, preferred_element_type=jnp.float32).astype(
        jnp.bfloat16
    )
    mixed = attend(query, new_key, new_value, cache_keys, cache_values, lengths, mixing)
    head_rows = head_norm(mixed, head_gain)
    update = jnp.dot(head_rows, out_weight, preferred_element_type=jnp.float32)
    residual = (hidden.astype(jnp.float32) + update).astype(jnp.bfloat16)
    expert_input = root_scale(residual, second_gain).astype(jnp.bfloat16)
    experts = lax.axis_size("ep") // EXP_SPLIT
    capacity = max(2, 2 * count * TOP_K // experts)
    match = slot_tables(routes, experts, capacity)
    pick = jnp.sum(match.astype(jnp.int32), axis=2).astype(jnp.bfloat16)
    packed = jnp.dot(pick, expert_input, preferred_element_type=jnp.float32).astype(jnp.bfloat16)
    outgoing = jnp.repeat(packed.reshape(experts, capacity, D), EXP_SPLIT, axis=0)
    rows = lax.all_to_all(outgoing, "ep", split_axis=0, concat_axis=0, tiled=True)
    flat = rows.reshape(-1, rows.shape[2])
    result = expert_apply(flat, expert_gate, expert_up, expert_down)
    returned = lax.all_to_all(
        result.reshape(rows.shape), "ep", split_axis=0, concat_axis=0, tiled=True
    )
    halves = returned.astype(jnp.float32).reshape(experts, EXP_SPLIT, capacity, D)
    expert_out = jnp.sum(halves, axis=1).reshape(experts * capacity, D)
    weighting = jnp.sum(jnp.where(match, route_weight[None, :, :], 0.0), axis=2).T
    routed = jnp.dot(weighting, expert_out, precision=lax.Precision.HIGHEST)
    layer_out = (residual.astype(jnp.float32) + routed).astype(jnp.bfloat16)
    return (layer_out, new_key, new_value)


def solution(mesh):
    return jax.shard_map(
        per_device,
        mesh=mesh,
        in_specs=(
            P("ep", None),
            P("ep", None, None),
            P("ep", None, None),
            P("ep"),
            P(),
            P(),
            P(),
            P(),
            P(),
            P(),
            P(),
            P(),
            P("ep", None),
            P("ep", None),
            P("ep", None, None),
            P("ep", None, None),
            P("ep", None, None),
        ),
        out_specs=(P("ep", None), P("ep", None), P("ep", None)),
        check_vma=False,
    )
```

profile of v0, /device:TPU:0, one launch (start us, length us, event | category | flops | bytes accessed | tf_op | source)
XLA Modules:
  0.0 132.3 jit_solution(4276068016359851897)
XLA Ops:
  0.6 0.0 copy-start
  0.6 1.1 fusion.22
  1.8 0.0 copy-start.12
  1.8 3.2 %convolution_convert_fusion.2 = bf16[32,1024]{1,0:T(8,128)(2,1)S(1)} fusion(bf16[2048,1024]{1,0:T(8,128)(2,1)} %param.22, bf16[32,2048]{1,0:T(8,128)(2,1)} %param.17, f32[2048]{0:T(1024)} %param.21, f32[32]{0:T(128)S(1)} %add_rsqrt_fusion.2), kind=kOutput, calls=%fused_computation.17 | convolution fusion | flops 134512640 | bytes 4399232 | tf_op jit(solution)/shard_map/dot_general | solution.py:99
  5.0 0.1 reshape.112
  5.1 0.0 copy-done.12
  5.1 0.1 iota_compare_fusion.1
  5.2 0.0 copy-start.2
  5.2 0.0 copy-start.4
  5.2 0.0 copy-start.6
  5.3 12.0 %copy.41 = bf16[32,1024,128]{1,2,0:T(8,128)(2,1)} copy(bf16[32,1024,128]{2,1,0:T(8,128)(2,1)} %param.18) | data formatting | bytes 16777216 | tf_op args[1]
  17.3 0.0 copy-done.2
  17.3 0.0 copy-done.4
  17.3 0.0 copy-done.6
  17.3 0.3 convolution_convert_fusion.4
  17.5 0.0 copy-start.7
  17.5 0.1 reshape.128
  17.6 0.2 fusion.28
  17.8 4.7 %bitcast_reduce_fusion = (f32[32,8,2]{1,2,0:T(2,128)S(1)}, f32[32,2,8,1024]{3,2,1,0:T(8,128)S(1)}) fusion(pred[32,1024]{1,0:T(8,128)(4,1)S(1)} %iota_compare_fusion.1, bf16[32,1024,2,64]{1,3,2,0:T(8,128)(2,1)} %bitcast.79, bf16[32,8,2,64]{3,2,1,0:T(2,128)(2,1)S(1)} %reshape.112), kind=kOutput, calls=%fused_computation.9 | convolution fusion | flops 68681216 | bytes 10586112 | tf_op jit(solution)/shard_map/shmd,slmd->shml/dot_general | solution.py:40
  22.5 0.0 copy-done.7
  22.6 0.7 fusion.5
  23.2 0.1 fusion.39
  23.3 0.0 copy-start.5
  23.3 0.0 copy-start.10
  23.3 0.6 fusion.4
  24.0 0.4 copy-done.5
  24.3 0.9 fusion.44
  25.2 0.0 copy-done.10
  25.2 0.0 copy-start.13
  25.2 0.0 copy-start.1
  25.3 4.9 %multiply_reduce_fusion.1 = (f32[32,8]{1,0:T(8,128)S(1)}, f32[32,8,128]{2,1,0:T(8,128)S(1)}) fusion(f32[32,128]{1,0:T(8,128)S(1)} %get-tuple-element.7, f32[32,8]{1,0:T(8,128)S(1)} %bitcast.84, bf16[32,1024,128]{2,1,0:T(8,128)(2,1)} %param.19, f32[32,8,2,1024]{3,1,2,0:T(8,128)S(1)} %fusion.4, f32[8]{0:T(128)S(1)} %copy-done.10), kind=kOutput, calls=%fused_computation.49 | convolution fusion | flops 68026112 | bytes 10635296 | tf_op jit(solution)/shard_map/shl,sle->she/dot_general | solution.py:58
  30.2 0.0 copy-done.13
  30.2 0.1 multiply_convert_fusion.2
  30.3 0.0 copy-done.1
  30.3 0.0 copy-start.9
  30.3 0.0 copy-start.8
  30.3 0.9 multiply_reduce_fusion
  31.3 0.0 copy-done.9
  31.3 0.1 copy.44
  31.4 0.1 eq.29
  31.5 0.1 fusion.34
  31.6 0.2 reduce_window_sum.11
  31.8 0.2 select_reduce_fusion.1
  31.9 0.1 reduce_sum.78
  32.1 0.1 copy.45
  32.1 0.1 convert_reduce_fusion.1
  32.2 0.0 copy-done.8
  32.3 0.5 convolution_convert_fusion.1
  32.7 0.4 reshape.115
  33.2 1.2 broadcast_in_dim.26
  34.4 41.3 %all_to_all.10 = bf16[128,4,2048]{2,1,0:T(4,128)(2,1)S(1)} all-to-all(bf16[128,4,2048]{2,1,0:T(4,128)(2,1)S(1)} %bitcast.80), channel_id=1, replica_groups=mesh['ep'=128] {'ep'}, dimensions={0} | all-to-all | bytes 4194304 | tf_op jit(solution)/shard_map/all_to_all | solution.py:115
  75.8 2.1 %reshape.117 = bf16[512,2048]{1,0:T(8,128)(2,1)} reshape(bf16[128,4,2048]{2,1,0:T(4,128)(2,1)S(1)} %all_to_all.10) | data formatting | bytes 4194304 | tf_op jit(solution)/shard_map/reshape | solution.py:116
  77.8 3.5 %fusion.13 = f32[512,256]{1,0:T(8,128)} fusion(bf16[512,2048]{1,0:T(8,128)(2,1)} %reshape.117, bf16[1,2048,256]{2,1,0:T(8,128)(2,1)} %param.31), kind=kOutput, calls=%fused_computation.27 | convolution fusion | flops 536870912 | bytes 3670016 | tf_op jit(solution)/shard_map/dot_general | solution.py:72
  81.3 0.0 copy-done
  81.3 0.0 copy-done.3
  81.3 5.0 %convolution_convert_fusion = bf16[512,2048]{1,0:T(8,128)(2,1)} fusion(bf16[512,2048]{1,0:T(8,128)(2,1)S(1)} %copy-done.3, bf16[1,256,2048]{2,1,0:T(8,128)(2,1)S(1)} %copy-done, bf16[1,2048,256]{2,1,0:T(8,128)(2,1)} %param.32, f32[512,256]{1,0:T(8,128)} %fusion.13), kind=kOutput, calls=%fused_computation.1 | convolution fusion | flops 1075576832 | bytes 6815744 | tf_op jit(solution)/shard_map/dot_general | solution.py:75
  86.4 4.1 %reshape.118 = bf16[128,4,2048]{2,1,0:T(4,128)(2,1)} reshape(bf16[512,2048]{1,0:T(8,128)(2,1)} %convolution_convert_fusion) | data formatting | bytes 4194304 | tf_op jit(solution)/shard_map/reshape | solution.py:119
  90.5 5.0 %all-to-all-start.1 = ((bf16[128,4,2048]{2,1,0:T(4,128)(2,1)}), bf16[128,4,2048]{2,1,0:T(4,128)(2,1)S(1)}, u32[]{:S(2)}, u32[]{:S(2)}) async-start(bf16[128,4,2048]{2,1,0:T(4,128)(2,1)} %reshape.118), calls=%async_computation.1 | async-start | bytes 4194304 | tf_op jit(solution)/shard_map/all_to_all | solution.py:118
  95.5 0.0 copy-done.11
  95.5 0.1 select_reduce_fusion
  95.6 30.1 %all-to-all-done.1 = bf16[128,4,2048]{2,1,0:T(4,128)(2,1)S(1)} async-done(((bf16[128,4,2048]{2,1,0:T(4,128)(2,1)}), bf16[128,4,2048]{2,1,0:T(4,128)(2,1)S(1)}, u32[]{:S(2)}, u32[]{:S(2)}) %all-to-all-start.1) | async-done | bytes 2097184 | tf_op jit(solution)/shard_map/all_to_all | solution.py:118
  125.6 2.7 %convert_reduce_fusion = f32[64,4,2048]{2,1,0:T(4,128)} fusion(bf16[128,4,2048]{2,1,0:T(4,128)(2,1)S(1)} %all-to-all-done.1), kind=kLoop, calls=%fused_computation | loop fusion | flops 1572864 | bytes 4194304 | tf_op jit(solution)/shard_map/reduce_sum | solution.py:122
  128.3 2.0 %reshape.121 = f32[256,2048]{1,0:T(8,128)S(1)} reshape(f32[64,4,2048]{2,1,0:T(4,128)} %convert_reduce_fusion) | data formatting | bytes 4194304 | tf_op jit(solution)/shard_map/reshape | solution.py:122
  130.3 2.0 %fusion.2 = bf16[32,2048]{1,0:T(8,128)(2,1)} fusion(f32[32,2048]{1,0:T(8,128)S(1)} %get-tuple-element.12, f32[256,32]{0,1:T(8,128)S(1)} %select_reduce_fusion, f32[256,2048]{1,0:T(8,128)S(1)} %reshape.121), kind=kOutput, calls=%fused_computation.7 | convolution fusion | flops 201457664 | bytes 2523136 | tf_op jit(solution)/shard_map/dot_general | solution.py:124
  (8 shorter events, 0.1 us)
Async XLA Ops:
  0.6 80.7 %copy-start = (bf16[1,256,2048]{2,1,0:T(8,128)(2,1)S(1)}, bf16[1,256,2048]{2,1,0:T(8,128)(2,1)}, u32[]{:S(2)}) copy-start(bf16[1,256,2048]{2,1,0:T(8,128)(2,1)} %param.33) | copy-start | bytes 3145732
  1.8 3.3 %copy-start.12 = (s32[32]{0:T(128)S(1)}, s32[32]{0:T(128)}, u32[]{:S(2)}) copy-start(s32[32]{0:T(128)} %param.20) | copy-start | bytes 388
  5.2 12.0 %copy-start.2 = (bf16[32,2048]{1,0:T(8,128)(2,1)S(1)}, bf16[32,2048]{1,0:T(8,128)(2,1)}, u32[]{:S(2)}) copy-start(bf16[32,2048]{1,0:T(8,128)(2,1)} %param.17) | copy-start | bytes 393220
  5.2 12.0 %copy-start.4 = (bf16[2048,128]{1,0:T(8,128)(2,1)S(1)}, bf16[2048,128]{1,0:T(8,128)(2,1)}, u32[]{:S(2)}) copy-start(bf16[2048,128]{1,0:T(8,128)(2,1)} %param.23) | copy-start | bytes 1572868
  5.2 12.0 %copy-start.6 = (f32[2048]{0:T(1024)S(1)}, f32[2048]{0:T(1024)}, u32[]{:S(2)}) copy-start(f32[2048]{0:T(1024)} %param.21) | copy-start | bytes 24580
  17.5 5.0 %copy-start.7 = (bf16[32,128]{1,0:T(8,128)(2,1)}, bf16[32,128]{1,0:T(8,128)(2,1)S(1)}, u32[]{:S(2)}) copy-start(bf16[32,128]{1,0:T(8,128)(2,1)S(1)} %convolution_convert_fusion.4) | copy-start | bytes 24580
  23.3 1.0 copy-start.5
  23.3 1.9 %copy-start.10 = (f32[8]{0:T(128)S(1)}, f32[8]{0:T(128)}, u32[]{:S(2)}) copy-start(f32[8]{0:T(128)} %param.25) | copy-start | bytes 100
  25.2 5.0 %copy-start.13 = (f32[128]{0:T(128)S(1)}, f32[128]{0:T(128)}, u32[]{:S(2)}) copy-start(f32[128]{0:T(128)} %param.26) | copy-start | bytes 1540
  25.2 5.1 %copy-start.1 = (bf16[1024,2048]{1,0:T(8,128)(2,1)S(1)}, bf16[1024,2048]{1,0:T(8,128)(2,1)}, u32[]{:S(2)}) copy-start(bf16[1024,2048]{1,0:T(8,128)(2,1)} %param.27) | copy-start | bytes 12582916
  30.3 1.0 copy-start.9
  30.3 1.9 %copy-start.8 = (f32[2048]{0:T(1024)S(1)}, f32[2048]{0:T(1024)}, u32[]{:S(2)}) copy-start(f32[2048]{0:T(1024)} %param.28) | copy-start | bytes 24580
  77.8 3.5 %copy-start.3 = (bf16[512,2048]{1,0:T(8,128)(2,1)S(1)}, bf16[512,2048]{1,0:T(8,128)(2,1)}, u32[]{:S(2)}) copy-start(bf16[512,2048]{1,0:T(8,128)(2,1)} %reshape.117) | copy-start | bytes 6291460
  90.5 5.0 %copy-start.11 = (f32[32,4]{0,1:T(4,128)S(1)}, f32[32,4]{0,1:T(4,128)}, u32[]{:S(2)}) copy-start(f32[32,4]{0,1:T(4,128)} %param.30) | copy-start | bytes 1540
  90.5 35.1 %all-to-all-start.1 = ((bf16[128,4,2048]{2,1,0:T(4,128)(2,1)}), bf16[128,4,2048]{2,1,0:T(4,128)(2,1)S(1)}, u32[]{:S(2)}, u32[]{:S(2)}) async-start(bf16[128,4,2048]{2,1,0:T(4,128)(2,1)} %reshape.118), calls=%async_computation.1 | async-start | bytes 4194304 | tf_op jit(solution)/shard_map/all_to_all | solution.py:118
where the time goes:
time: 133 us; the launch traced here: 132 us
  blocking collectives  41.3 us (31%)
  waiting for transfers between devices  30.1 us (23%)
  matrix products  26 us (20%)
  local copies, waits for them, and re-layouts  22.9 us (17%)
  other arithmetic  6.08 us (5%)
  starting transfers between devices  4.96 us (4%)
    all_to_all x1, blocking collectives, per_device(): lax.all_to_all(outgoing, 'ep', split_axis=0, concat_axis=0, tiled=True)  41.3 us
    all_to_all x1, waiting for transfers between devices, per_device(): lax.all_to_all(result.reshape(rows.shape), 'ep', split_axis=0, concat_axi...  30.1 us
    unnamed x30, local copies, waits for them, and re-layouts  12.6 us
    dot_general x1, matrix products, expert_apply(): jnp.dot(inner, expert_down[0], preferred_element_type=jnp.float32)  5.02 us
    all_to_all x1, starting transfers between devices, per_device(): lax.all_to_all(result.reshape(rows.shape), 'ep', split_axis=0, concat_axi...  4.96 us
    dot_general x1, matrix products, attend(): jnp.einsum('shl,sle->she', contrast, cache_values, preferred_element_type...  4.9 us
    dot_general x1, matrix products, attend(): jnp.einsum('shmd,slmd->shml', queries, keys, preferred_element_type=jnp.f...  4.69 us
    reshape x1, local copies, waits for them, and re-layouts, per_device(): result.reshape(rows.shape)  4.12 us
  transfers between devices with their start and end apart: 1, of which 1 were waited for; matrix products, arithmetic and copies ran while one was open for 0% of the time, Pallas kernels for 0%

commit v1 on v0

v1 whole, which is shorter than its diff:
```python
import jax
import jax.numpy as jnp
from jax import lax
from jax.experimental import pallas as pl
from jax.experimental.pallas import tpu as pltpu
from jax.sharding import PartitionSpec as P

D = 2048
HALF = D // 2
HEADS = 8
DK = 64
DV = 128
EXP_SPLIT = 2
TOP_K = 4
CAP = 4
ROWS = 8
BLOCK = 256
GROUP = 4
WCHUNKS = 4

epsilon = 1e-06
MIB = 1024 * 1024


def root_factor(values):
    return lax.rsqrt(jnp.mean(values * values, axis=-1, keepdims=True) + epsilon)


def routing_tables(routes, route_weight, pick, weighting_out):
    count = routes.shape[1]
    slots = pick.shape[0]
    f32 = jnp.float32
    across = [routes[j : j + 1, :].astype(f32) for j in range(TOP_K)]
    rows_at = lax.broadcasted_iota(jnp.int32, (count, count), 0)
    columns_at = lax.broadcasted_iota(jnp.int32, (count, count), 1)

    def turn(row):
        return jnp.sum(jnp.where(rows_at == columns_at, row, 0.0), axis=1, keepdims=True)

    down = [turn(row) for row in across]
    same = down[0] == across[0]
    for j in range(1, TOP_K):
        same = same | (down[0] == across[j])
    shared = jnp.where(same, 1.0, 0.0)
    rank_across = jnp.sum(jnp.where(rows_at < columns_at, shared, 0.0), axis=0, keepdims=True)
    rank_down = turn(rank_across)

    slot = lax.broadcasted_iota(jnp.int32, (slots, count), 0)
    expert = (slot // ROWS).astype(f32)
    hit = expert == across[0]
    for j in range(1, TOP_K):
        hit = hit | (expert == across[j])
    chosen = jnp.where(hit & ((slot % CAP).astype(f32) == rank_across), 1.0, 0.0)
    upper = (slot // CAP) % 2 == 1
    pick[...] = jnp.concatenate(
        [jnp.where(upper, 0.0, chosen), jnp.where(upper, chosen, 0.0)], axis=1
    ).astype(jnp.bfloat16)

    slot = lax.broadcasted_iota(jnp.int32, (count, slots), 1)
    expert = (slot // ROWS).astype(f32)
    weighting = jnp.zeros((count, slots), f32)
    for j in range(TOP_K):
        weighting = weighting + jnp.where(
            expert == down[j], turn(route_weight[j : j + 1, :]), 0.0
        )
    weighting = jnp.where((slot % CAP).astype(f32) == rank_down, weighting, 0.0)
    upper = (slot // CAP) % 2 == 1
    whole = jnp.concatenate(
        [jnp.where(upper, 0.0, weighting), jnp.where(upper, weighting, 0.0)], axis=0
    )
    coarse = whole.astype(jnp.bfloat16)
    fine = (whole - coarse.astype(f32)).astype(jnp.bfloat16)
    weighting_out[...] = jnp.concatenate([coarse, fine], axis=0)


def front_kernel(
    lengths_hbm,
    mixing_hbm,
    hidden_hbm,
    first_gain_hbm,
    head_gain_hbm,
    second_gain_hbm,
    routes_hbm,
    route_weight_hbm,
    wq_hbm,
    wk_hbm,
    wv_hbm,
    wo_hbm,
    keys_hbm,
    values_hbm,
    packed,
    residual_out,
    new_key_out,
    new_value_out,
    weighting_out,
    lengths,
    mixing,
    hidden,
    first_gain,
    head_gain,
    second_gain,
    routes,
    route_weight,
    wq,
    wk,
    wv,
    wo,
    kbuf,
    vbuf,
    queries,
    own_key,
    own_value,
    mixed,
    pick,
    order,
    ssem,
    wsem,
    osem,
    ksem,
    vsem,
):
    count = hidden.shape[0]
    span = keys_hbm.shape[1]
    blocks = span // BLOCK
    groups = count // GROUP
    part = D // WCHUNKS

    def weight_copies(i):
        rows = pl.ds(i * part, part)
        return [
            pltpu.make_async_copy(source.at[rows], target.at[rows], wsem.at[n, i])
            for n, (source, target) in enumerate(((wq_hbm, wq), (wk_hbm, wk), (wv_hbm, wv)))
        ]

    small = [
        pltpu.make_async_copy(source, target, ssem.at[n])
        for n, (source, target) in enumerate(
            (
                (lengths_hbm, lengths),
                (hidden_hbm, hidden),
                (first_gain_hbm, first_gain),
                (routes_hbm, routes),
                (route_weight_hbm, route_weight),
                (mixing_hbm, mixing),
                (head_gain_hbm, head_gain),
                (second_gain_hbm, second_gain),
            )
        )
    ]
    for copy in small:
        copy.start()
    for i in range(WCHUNKS):
        for copy in weight_copies(i):
            copy.start()
    small[0].wait()

    def blocks_of(i):
        return (lengths[i] + (BLOCK - 1)) // BLOCK

    place = jnp.int32(0)
    for b in range(1, blocks + 1):
        for i in range(count):
            order[place] = jnp.int32(i)
            place = place + (blocks_of(i) == b).astype(jnp.int32)

    def cache_copies(g, n):
        copies = []
        rows = pl.ds(0, n * BLOCK)
        for i in range(GROUP):
            at = g * GROUP + i
            s = order[at]
            copies.append(
                pltpu.make_async_copy(keys_hbm.at[s, rows], kbuf.at[at, rows], ksem.at[at])
            )
            copies.append(
                pltpu.make_async_copy(values_hbm.at[s, rows], vbuf.at[at, rows], vsem.at[at])
            )
        return copies

    def start_group(g, carry):
        need = blocks_of(order[g * GROUP + GROUP - 1])
        for n in range(1, blocks + 1):

            @pl.when(need == n)
            def _():
                for copy in cache_copies(g, n):
                    copy.start()

        return carry

    lax.fori_loop(0, groups, start_group, 0)
    wo_copy = pltpu.make_async_copy(wo_hbm, wo, osem)
    wo_copy.start()
    for copy in small[1:]:
        copy.wait()
    routing_tables(routes, route_weight, pick, weighting_out)

    hid = hidden[...].astype(jnp.float32)
    normed = (hid * root_factor(hid) * first_gain[...]).astype(jnp.bfloat16)
    q = jnp.zeros((count, HEADS * 2 * DK), jnp.float32)
    k = jnp.zeros((count, 2 * DK), jnp.float32)
    v = jnp.zeros((count, DV), jnp.float32)
    for i in range(WCHUNKS):
        for copy in weight_copies(i):
            copy.wait()
        rows = slice(i * part, (i + 1) * part)
        left = normed[:, rows]
        q = q + jnp.dot(left, wq[rows], preferred_element_type=jnp.float32)
        k = k + jnp.dot(left, wk[rows], preferred_element_type=jnp.float32)
        v = v + jnp.dot(left, wv[rows], preferred_element_type=jnp.float32)
    q = q.astype(jnp.bfloat16).astype(jnp.float32) * DK ** (-0.5)
    k = k.astype(jnp.bfloat16)
    v = v.astype(jnp.bfloat16)
    new_key_out[...] = k
    new_value_out[...] = v
    own_key[...] = k.astype(jnp.float32)
    own_value[...] = v.astype(jnp.float32)
    for h in range(HEADS):
        queries[pl.ds(h, count, stride=HEADS), :] = q[:, h * 2 * DK : (h + 1) * 2 * DK]

    head_at = lax.broadcasted_iota(jnp.int32, (HEADS, 1), 0)
    mix = jnp.zeros((HEADS, 1), jnp.float32)
    for h in range(HEADS):
        mix = jnp.where(head_at == h, mixing[h], mix)
    low = lax.broadcasted_iota(jnp.int32, (HEADS, 2 * DK), 1) < DK

    def attend_group(g, n):
        for copy in cache_copies(g, n):
            copy.wait()
        wide = n * BLOCK
        column = lax.broadcasted_iota(jnp.int32, (2 * HEADS, wide), 1)
        for i in range(GROUP):
            at = g * GROUP + i
            s = order[at]
            rows = queries[pl.ds(pl.multiple_of(s * HEADS, HEADS), HEADS), :]
            both = jnp.concatenate([jnp.where(low, rows, 0.0), jnp.where(low, 0.0, rows)], axis=0)
            own = jnp.sum(both * own_key[pl.ds(s, 1), :], axis=-1, keepdims=True)
            scores = lax.dot_general(
                both.astype(jnp.bfloat16),
                kbuf[at, :wide, :],
                (((1,), (1,)), ((), ())),
                preferred_element_type=jnp.float32,
            )
            scores = jnp.where(column < lengths[s], scores, -jnp.inf)
            highest = jnp.maximum(jnp.max(scores, axis=-1, keepdims=True), own)
            weights = jnp.exp(scores - highest)
            own_weights = jnp.exp(own - highest)
            total = jnp.sum(weights, axis=-1, keepdims=True) + own_weights
            first = 1.0 / total[:HEADS]
            second = mix / total[HEADS:]
            contrast = (weights[:HEADS] * first - weights[HEADS:] * second).astype(jnp.bfloat16)
            own_contrast = (own_weights[:HEADS] * first - own_weights[HEADS:] * second).astype(
                jnp.bfloat16
            )
            out = jnp.dot(contrast, vbuf[at, :wide, :], preferred_element_type=jnp.float32)
            out = out + own_contrast.astype(jnp.float32) * own_value[pl.ds(s, 1), :]
            mixed[pl.ds(pl.multiple_of(s * HEADS, HEADS), HEADS), :] = out

    def run_group(g, carry):
        need = blocks_of(order[g * GROUP + GROUP - 1])
        for n in range(1, blocks + 1):

            @pl.when(need == n)
            def _():
                attend_group(g, n)

        return carry

    lax.fori_loop(0, groups, run_group, 0)

    pieces = []
    for h in range(HEADS):
        rows = mixed[pl.ds(h, count, stride=HEADS), :]
        pieces.append((rows * root_factor(rows) * head_gain[...]).astype(jnp.bfloat16))
    head_rows = jnp.concatenate(pieces, axis=1)
    wo_copy.wait()
    update = jnp.dot(head_rows, wo[...], preferred_element_type=jnp.float32)
    residual = (hid + update).astype(jnp.bfloat16)
    residual_out[...] = residual
    res = residual.astype(jnp.float32)
    expert_input = (res * root_factor(res) * second_gain[...]).astype(jnp.bfloat16)

    stacked = jnp.concatenate([expert_input[:, :HALF], expert_input[:, HALF:]], axis=0)
    sent = jnp.dot(pick[...], stacked, preferred_element_type=jnp.float32).astype(jnp.bfloat16)
    packed[...] = sent.reshape(packed.shape)


def front(
    lengths,
    mixing,
    hidden,
    first_gain,
    head_gain,
    second_gain,
    routes,
    route_weight,
    wq,
    wk,
    wv,
    wo,
    keys,
    values,
    experts,
):
    count = hidden.shape[0]
    slots = experts * ROWS
    vmem = pl.BlockSpec(memory_space=pltpu.VMEM)
    hbm = pl.BlockSpec(memory_space=pltpu.HBM)
    bf16 = jnp.bfloat16
    f32 = jnp.float32
    operands = (
        lengths,
        mixing,
        hidden,
        first_gain.reshape(1, D),
        head_gain.reshape(1, DV),
        second_gain.reshape(1, D),
        routes.T,
        route_weight.T,
        wq,
        wk,
        wv,
        wo,
        keys,
        values,
    )
    return pl.pallas_call(
        front_kernel,
        out_shape=(
            jax.ShapeDtypeStruct((experts, ROWS, HALF), bf16),
            jax.ShapeDtypeStruct((count, D), bf16),
            jax.ShapeDtypeStruct((count, 2 * DK), bf16),
            jax.ShapeDtypeStruct((count, DV), bf16),
            jax.ShapeDtypeStruct((4 * count, slots), bf16),
        ),
        in_specs=[hbm] * 14,
        out_specs=(vmem,) * 5,
        scratch_shapes=[
            pltpu.SMEM(lengths.shape, jnp.int32),
            pltpu.SMEM(mixing.shape, f32),
            pltpu.VMEM(hidden.shape, bf16),
            pltpu.VMEM((1, D), f32),
            pltpu.VMEM((1, DV), f32),
            pltpu.VMEM((1, D), f32),
            pltpu.VMEM((TOP_K, count), jnp.int32),
            pltpu.VMEM((TOP_K, count), f32),
            pltpu.VMEM(wq.shape, bf16),
            pltpu.VMEM(wk.shape, bf16),
            pltpu.VMEM(wv.shape, bf16),
            pltpu.VMEM(wo.shape, bf16),
            pltpu.VMEM(keys.shape, bf16),
            pltpu.VMEM(values.shape, bf16),
            pltpu.VMEM((count * HEADS, 2 * DK), f32),
            pltpu.VMEM((count, 2 * DK), f32),
            pltpu.VMEM((count, DV), f32),
            pltpu.VMEM((count * HEADS, DV), f32),
            pltpu.VMEM((slots, 2 * count), bf16),
            pltpu.SMEM((count + 1,), jnp.int32),
            pltpu.SemaphoreType.DMA((8,)),
            pltpu.SemaphoreType.DMA((3, WCHUNKS)),
            pltpu.SemaphoreType.DMA(()),
            pltpu.SemaphoreType.DMA((count,)),
            pltpu.SemaphoreType.DMA((count,)),
        ],
        compiler_params=pltpu.CompilerParams(vmem_limit_bytes=40 * MIB),
        cost_estimate=pl.CostEstimate(
            flops=20_000_000_000, transcendentals=0, bytes_accessed=25 * MIB
        ),
        name="front",
    )(*[pltpu.with_memory_space_constraint(x, pltpu.HBM) for x in operands])


def swap_halves(pairs):
    first = pairs[:, 0]
    second = pairs[:, 1]
    top = lax.broadcasted_iota(jnp.int32, first.shape, 1) < CAP
    low = jnp.where(top, first, pltpu.roll(second, CAP, 1))
    high = jnp.where(top, pltpu.roll(first, CAP, 1), second)
    return low, high


def expert_kernel(rows, gate_a, gate_b, up_a, up_b, down_a, down_b, result):
    sources = rows.shape[0]
    count = sources * CAP
    f32 = jnp.float32
    pairs = rows[...].astype(f32).reshape(sources // 2, 2, ROWS, HALF)
    low, high = swap_halves(pairs)
    low = low.reshape(count, HALF).astype(jnp.bfloat16)
    high = high.reshape(count, HALF).astype(jnp.bfloat16)

    def project(weight):
        return jnp.dot(low, weight[:HALF], preferred_element_type=f32) + jnp.dot(
            high, weight[HALF:], preferred_element_type=f32
        )

    inner = []
    for gate_w, up_w in ((gate_a, up_a), (gate_b, up_b)):
        gate = project(gate_w)
        inner.append((gate / (1.0 + jnp.exp(-gate)) * project(up_w)).astype(jnp.bfloat16))
    halves = []
    for j in range(2):
        columns = slice(j * HALF, (j + 1) * HALF)
        half = jnp.dot(inner[0], down_a[:, columns], preferred_element_type=f32) + jnp.dot(
            inner[1], down_b[:, columns], preferred_element_type=f32
        )
        halves.append(half.reshape(sources // 2, 1, ROWS, HALF))
    first, second = swap_halves(jnp.concatenate(halves, axis=1))
    result[...] = (
        jnp.stack([first, second], axis=1).reshape(sources, ROWS, HALF).astype(jnp.bfloat16)
    )


def expert(rows, *weights):
    return pl.pallas_call(
        expert_kernel,
        out_shape=jax.ShapeDtypeStruct(rows.shape, rows.dtype),
        compiler_params=pltpu.CompilerParams(vmem_limit_bytes=32 * MIB),
        cost_estimate=pl.CostEstimate(
            flops=3_000_000_000, transcendentals=0, bytes_accessed=8 * MIB
        ),
        name="expert",
    )(rows, *weights)


def combine_kernel(returned, residual, weighting, out):
    count = residual.shape[0]
    values = returned[...].reshape(returned.shape[0] * ROWS, HALF)
    both = jnp.dot(weighting[...], values, preferred_element_type=jnp.float32)
    routed = both[: 2 * count] + both[2 * count :]
    res = residual[...].astype(jnp.float32)
    out[:, :HALF] = (res[:, :HALF] + routed[:count]).astype(jnp.bfloat16)
    out[:, HALF:] = (res[:, HALF:] + routed[count:]).astype(jnp.bfloat16)


def combine(returned, residual, weighting):
    return pl.pallas_call(
        combine_kernel,
        out_shape=jax.ShapeDtypeStruct(residual.shape, residual.dtype),
        compiler_params=pltpu.CompilerParams(vmem_limit_bytes=16 * MIB),
        name="combine",
    )(returned, residual, weighting)


def per_device(
    hidden,
    cache_keys,
    cache_values,
    lengths,
    first_gain,
    query_weight,
    key_weight,
    value_weight,
    mixing,
    head_gain,
    out_weight,
    second_gain,
    routes,
    route_weight,
    expert_gate,
    expert_up,
    expert_down,
):
    devices = lax.axis_size("ep")
    experts = devices // EXP_SPLIT
    partners = [(i, i ^ 1) for i in range(devices)]
    lanes = [[e * EXP_SPLIT + j for e in range(experts)] for j in range(EXP_SPLIT)]
    peer = [lax.ppermute(w[0], "ep", partners) for w in (expert_gate, expert_up, expert_down)]

    packed, residual, new_key, new_value, weighting = front(
        lengths,
        mixing,
        hidden,
        first_gain,
        head_gain,
        second_gain,
        routes,
        route_weight,
        query_weight,
        key_weight,
        value_weight,
        out_weight,
        cache_keys,
        cache_values,
        experts,
    )
    rows = lax.all_to_all(packed, "ep", 0, 0, axis_index_groups=lanes, tiled=True)
    result = expert(
        rows, expert_gate[0], peer[0], expert_up[0], peer[1], expert_down[0], peer[2]
    )
    returned = lax.all_to_all(result, "ep", 0, 0, axis_index_groups=lanes, tiled=True)
    layer_out = combine(returned, residual, weighting)
    return (layer_out, new_key, new_value)


def solution(mesh):
    return jax.shard_map(
        per_device,
        mesh=mesh,
        in_specs=(
            P("ep", None),
            P("ep", None, None),
            P("ep", None, None),
            P("ep"),
            P(),
            P(),
            P(),
            P(),
            P(),
            P(),
            P(),
            P(),
            P("ep", None),
            P("ep", None),
            P("ep", None, None),
            P("ep", None, None),
            P("ep", None, None),
        ),
        out_specs=(P("ep", None), P("ep", None), P("ep", None)),
        check_vma=False,
    )
```

time: 133 us -> 77 us (0.58)
  waiting for transfers between devices: 30.1 us -> 0.01 us
  matrix products: 26 us -> 0 us
  local copies, waits for them, and re-layouts: 22.9 us -> 0.01 us
  Pallas kernels: 0 us -> 21.9 us
  blocking collectives: 41.3 us -> 53.2 us
  other arithmetic: 6.08 us -> 0 us
  starting transfers between devices: 4.96 us -> 0.67 us
    all_to_all x1 -> x0, waiting for transfers between devices: 30.1 us -> none  [per_device(): lax.all_to_all(result.reshape(rows.shape), 'ep', split_axis=0, concat_axi...]
    dot_general x11 -> x0, matrix products: 26 us -> none  [the longest x1 5.02 us: expert_apply(): jnp.dot(inner, expert_down[0], preferred_element_type=jnp.float32)]
    pallas_call x0 -> x3, Pallas kernels: none -> 21.9 us  [the longest x1 19 us: front(): pl.pallas_call(front_kernel, out_shape=(jax.ShapeDtypeStruct((experts, RO...]
    unnamed x30 -> x6, local copies, waits for them, and re-layouts: 12.6 us -> 0.01 us
    all_to_all x1 -> x2, blocking collectives: 41.3 us -> 53.2 us  [the longest x1 30.6 us: per_device(): lax.all_to_all(packed, 'ep', 0, 0, axis_index_groups=lanes, tiled=True)]
    reshape x6 -> x0, local copies, waits for them, and re-layouts: 8.81 us -> none  [the longest x1 4.12 us: per_device(): result.reshape(rows.shape)]
    all_to_all x1 -> x0, starting transfers between devices: 4.96 us -> none  [per_device(): lax.all_to_all(result.reshape(rows.shape), 'ep', split_axis=0, concat_axi...]
    reduce_sum x6 -> x0, other arithmetic: 4.86 us -> none  [the longest x1 2.69 us: per_device(): expert_out = jnp.sum(halves, axis=1).reshape(experts * capacity, D)]
  transfers between devices with their start and end apart: 1 -> 3, of which waited for: 1 -> 0; matrix products, arithmetic and copies ran while one was open for 0% -> 0% of each run, Pallas kernels for 0% -> 25%
where the time goes in v1:
time: 77 us; the launch traced here: 76.5 us
  blocking collectives  53.2 us (69%)
  Pallas kernels  21.9 us (28%)
    all_to_all x1, blocking collectives, per_device(): lax.all_to_all(packed, 'ep', 0, 0, axis_index_groups=lanes, tiled=True)  30.6 us
    all_to_all x1, blocking collectives, per_device(): lax.all_to_all(result, 'ep', 0, 0, axis_index_groups=lanes, tiled=True)  22.6 us
    pallas_call x1, Pallas kernels, front(): pl.pallas_call(front_kernel, out_shape=(jax.ShapeDtypeStruct((experts, RO...  19 us
    pallas_call x1, Pallas kernels, expert(): pl.pallas_call(expert_kernel, out_shape=jax.ShapeDtypeStruct(rows.shape,...  1.96 us
  transfers between devices with their start and end apart: 3, of which 0 were waited for; matrix products, arithmetic and copies ran while one was open for 0% of the time, Pallas kernels for 25%

profile of v1, /device:TPU:0, one launch (start us, length us, event | category | flops | bytes accessed | tf_op | source)
XLA Modules:
  0.0 76.5 jit_solution(14226630367900638930)
XLA Ops:
  0.6 0.1 collective-permute-start
  0.7 0.5 collective-permute-start.1
  1.2 0.1 collective-permute-start.2
  1.3 0.0 copy-start
  1.3 0.0 copy-start.1
  1.3 0.0 copy-start.2
  1.3 19.0 %front.1 = (bf16[64,8,1024]{2,1,0:T(8,128)(2,1)S(1)}, bf16[32,2048]{1,0:T(8,128)(2,1)S(1)}, bf16[32,128]{1,0:T(8,128)(2,1)}, bf16[32,128]{1,0:T(8,128)(2,1)}, bf16[128,512]{1,0:T(8,128)(2,1)S(1)}) custom-call(s32[32]{0:T(128)} %lengths_hbm.1, f32[8]{0:T(128)} %mixing_hbm.1, bf16[32,2048]{1,0:T(8,128)(2,1)} %hidden_hbm.1, f32[1,2048]{1,0:T(1,128)} %bitcast.14, ...), custom_call_target="tpu_custom_call" | custom-call | flops 20000000000 | bytes 26214400 | tf_op jit(solution)/shard_map/front/pallas_call | solution.py:327
  20.3 30.6 %all_to_all.10.rows = bf16[64,8,1024]{2,1,0:T(8,128)(2,1)S(1)} all-to-all(bf16[64,8,1024]{2,1,0:T(8,128)(2,1)S(1)} %get-tuple-element.8), channel_id=1, replica_groups={{0,2,4,6,8,10,12,14,16,18,20,22,24,26,28,30,32,34,36,38,40,42,44,46,48,..., dimensions={0} | all-to-all | bytes 2097152 | tf_op jit(solution)/shard_map/all_to_all | solution.py:486
  50.9 0.0 collective-permute-done.gate_b
  50.9 0.0 collective-permute-done.1.up_b
  50.9 0.0 collective-permute-done.2.down_b
  50.9 0.0 copy-done
  50.9 0.0 copy-done.1
  50.9 0.0 copy-done.2
  50.9 2.0 %expert.1 = bf16[64,8,1024]{2,1,0:T(8,128)(2,1)S(1)} custom-call(bf16[64,8,1024]{2,1,0:T(8,128)(2,1)S(1)} %all_to_all.10.rows, bf16[2048,256]{1,0:T(8,128)(2,1)S(1)} %bitcast.9, bf16[2048,256]{1,0:T(8,128)(2,1)S(1)} %collective-permute-done.gate_b, bf16[2048,256]{1,0:T(8,128)(2,1)S(1)} %bitcast.11, bf16[2048,256]{1,0:T(8,128)(2,1)S(1)} %collective-permute-done.1.up_b, ...), custom_call_target="tpu_custom_call" | custom-call | flops 3000000000 | bytes 8388608 | tf_op jit(solution)/shard_map/expert/pallas_call | solution.py:414
  52.9 22.6 %all_to_all.11.returned = bf16[64,8,1024]{2,1,0:T(8,128)(2,1)S(1)} all-to-all(bf16[64,8,1024]{2,1,0:T(8,128)(2,1)S(1)} %expert.1), channel_id=1, replica_groups={{0,2,4,6,8,10,12,14,16,18,20,22,24,26,28,30,32,34,36,38,40,42,44,46,48,..., dimensions={0} | all-to-all | bytes 2097152 | tf_op jit(solution)/shard_map/all_to_all | solution.py:490
  75.5 1.0 %combine.1 = bf16[32,2048]{1,0:T(8,128)(2,1)} custom-call(bf16[64,8,1024]{2,1,0:T(8,128)(2,1)S(1)} %all_to_all.11.returned, bf16[32,2048]{1,0:T(8,128)(2,1)S(1)} %get-tuple-element.9.residual, bf16[128,512]{1,0:T(8,128)(2,1)S(1)} %get-tuple-element.10.weighting), custom_call_target="tpu_custom_call" | custom-call | tf_op jit(solution)/shard_map/combine/pallas_call | solution.py:436
Async XLA Ops:
  0.6 50.3 %collective-permute-start = (bf16[2048,256]{1,0:T(8,128)(2,1)}, bf16[2048,256]{1,0:T(8,128)(2,1)S(1)}, u32[]{:S(2)}, u32[]{:S(2)}) collective-permute-start(bf16[2048,256]{1,0:T(8,128)(2,1)} %bitcast.8), channel_id=1, source_target_pairs={{0,1},{1,0},{2,3},{3,2},{4,5},{5,4},{6,7},{7,6},{8,9},{9,8},{10,11... | collective-permute-start | bytes 3145736 | tf_op jit(solution)/shard_map/ppermute | solution.py:467
  0.7 50.2 %collective-permute-start.1 = (bf16[2048,256]{1,0:T(8,128)(2,1)}, bf16[2048,256]{1,0:T(8,128)(2,1)S(1)}, u32[]{:S(2)}, u32[]{:S(2)}) collective-permute-start(bf16[2048,256]{1,0:T(8,128)(2,1)} %bitcast.10), channel_id=1, source_target_pairs={{0,1},{1,0},{2,3},{3,2},{4,5},{5,4},{6,7},{7,6},{8,9},{9,8},{10,11... | collective-permute-start | bytes 3145736 | tf_op jit(solution)/shard_map/ppermute | solution.py:467
  1.2 49.7 %collective-permute-start.2 = (bf16[256,2048]{1,0:T(8,128)(2,1)}, bf16[256,2048]{1,0:T(8,128)(2,1)S(1)}, u32[]{:S(2)}, u32[]{:S(2)}) collective-permute-start(bf16[256,2048]{1,0:T(8,128)(2,1)} %bitcast.12), channel_id=1, source_target_pairs={{0,1},{1,0},{2,3},{3,2},{4,5},{5,4},{6,7},{7,6},{8,9},{9,8},{10,11... | collective-permute-start | bytes 3145736 | tf_op jit(solution)/shard_map/ppermute | solution.py:467
  1.3 49.6 %copy-start = (bf16[1,2048,256]{2,1,0:T(8,128)(2,1)S(1)}, bf16[1,2048,256]{2,1,0:T(8,128)(2,1)}, u32[]{:S(2)}) copy-start(bf16[1,2048,256]{2,1,0:T(8,128)(2,1)} %param.31) | copy-start | bytes 3145732
  1.3 49.6 %copy-start.1 = (bf16[1,2048,256]{2,1,0:T(8,128)(2,1)S(1)}, bf16[1,2048,256]{2,1,0:T(8,128)(2,1)}, u32[]{:S(2)}) copy-start(bf16[1,2048,256]{2,1,0:T(8,128)(2,1)} %param.32) | copy-start | bytes 3145732
  1.3 49.6 %copy-start.2 = (bf16[1,256,2048]{2,1,0:T(8,128)(2,1)S(1)}, bf16[1,256,2048]{2,1,0:T(8,128)(2,1)}, u32[]{:S(2)}) copy-start(bf16[1,256,2048]{2,1,0:T(8,128)(2,1)} %param.33) | copy-start | bytes 3145732

commit v2 on v1

--- a/solution.py
+++ b/solution.py
@@ -15,7 +15,7 @@
 CAP = 4
 ROWS = 8
 BLOCK = 256
-GROUP = 4
+GROUP = 8
 WCHUNKS = 4
 
 epsilon = 1e-06
@@ -111,6 +111,8 @@
     own_key,
     own_value,
     mixed,
+    own_scores,
+    scores_at,
     pick,
     order,
     ssem,
@@ -154,41 +156,59 @@
             copy.start()
     small[0].wait()
 
-    def blocks_of(i):
-        return (lengths[i] + (BLOCK - 1)) // BLOCK
-
-    place = jnp.int32(0)
-    for b in range(1, blocks + 1):
-        for i in range(count):
-            order[place] = jnp.int32(i)
-            place = place + (blocks_of(i) == b).astype(jnp.int32)
-
-    def cache_copies(g, n):
-        copies = []
+    def passed(i):
+        return [(lengths[i] > b * BLOCK).astype(jnp.int32) for b in range(1, blocks)]
+
+    starts = [jnp.int32(0)] + [jnp.int32(count)] * (blocks - 1)
+    for i in range(count):
+        more = passed(i)
+        starts = starts[:1] + [at - one for at, one in zip(starts[1:], more)]
+    for i in range(count):
+        more = passed(i)
+        place = starts[0]
+        for at, one in zip(starts[1:], more):
+            place = jnp.where(one > 0, at, place)
+        order[place] = jnp.int32(i)
+        kinds = [1] + more + [0]
+        starts = [at + (kinds[b] - kinds[b + 1]) for b, at in enumerate(starts)]
+
+    def group_blocks(g):
+        return 1 + sum(passed(order[g * GROUP + GROUP - 1]))
+
+    def cache_copies(source, target, sem, g, n):
         rows = pl.ds(0, n * BLOCK)
-        for i in range(GROUP):
-            at = g * GROUP + i
-            s = order[at]
-            copies.append(
-                pltpu.make_async_copy(keys_hbm.at[s, rows], kbuf.at[at, rows], ksem.at[at])
+        return [
+            pltpu.make_async_copy(
+                source.at[order[g * GROUP + i], rows],
+                target.at[g * GROUP + i, rows],
+                sem.at[g * GROUP + i],
             )
-            copies.append(
-                pltpu.make_async_copy(values_hbm.at[s, rows], vbuf.at[at, rows], vsem.at[at])
-            )
-        return copies
-
-    def start_group(g, carry):
-        need = blocks_of(order[g * GROUP + GROUP - 1])
-        for n in range(1, blocks + 1):
-
-            @pl.when(need == n)
-            def _():
-                for copy in cache_copies(g, n):
-                    copy.start()
-
-        return carry
-
-    lax.fori_loop(0, groups, start_group, 0)
+            for i in range(GROUP)
+        ]
+
+    def by_blocks(body):
+        def step(g, carry):
+            need = group_blocks(g)
+            for n in range(1, blocks + 1):
+
+                @pl.when(need == n)
+                def _():
+                    body(g, n)
+
+            return carry
+
+        lax.fori_loop(0, groups, step, 0)
+
+    def start_keys(g, n):
+        for copy in cache_copies(keys_hbm, kbuf, ksem, g, n):
+            copy.start()
+
+    def start_values(g, n):
+        for copy in cache_copies(values_hbm, vbuf, vsem, g, n):
+            copy.start()
+
+    by_blocks(start_keys)
+    by_blocks(start_values)
     wo_copy = pltpu.make_async_copy(wo_hbm, wo, osem)
     wo_copy.start()
     for copy in small[1:]:
@@ -223,25 +243,39 @@
     for h in range(HEADS):
         mix = jnp.where(head_at == h, mixing[h], mix)
     low = lax.broadcasted_iota(jnp.int32, (HEADS, 2 * DK), 1) < DK
-
-    def attend_group(g, n):
-        for copy in cache_copies(g, n):
+    pair = 2 * HEADS
+    lane_owner = lax.broadcasted_iota(jnp.int32, (2 * DK, GROUP * pair), 1) // pair
+
+    def score_group(g, n):
+        wide = n * BLOCK
+        both = []
+        for i in range(GROUP):
+            s = order[g * GROUP + i]
+            rows = queries[pl.ds(pl.multiple_of(s * HEADS, HEADS), HEADS), :]
+            both.append(
+                jnp.concatenate([jnp.where(low, rows, 0.0), jnp.where(low, 0.0, rows)], axis=0)
+            )
+            own_rows = both[i] * own_key[pl.ds(s, 1), :]
+            own_scores[g, i * pair : (i + 1) * pair, :] = own_rows
+        turned = jnp.concatenate(both, axis=0).T
+        spread = jnp.concatenate(
+            [jnp.where(lane_owner == i, turned, 0.0) for i in range(GROUP)], axis=0
+        ).astype(jnp.bfloat16)
+        for copy in cache_copies(keys_hbm, kbuf, ksem, g, n):
             copy.wait()
+        keys = jnp.concatenate([kbuf[g * GROUP + i, :wide, :] for i in range(GROUP)], axis=1)
+        scores_at[g, :, :wide] = jnp.dot(keys, spread, preferred_element_type=jnp.float32).T
+
+    def mix_group(g, n):
         wide = n * BLOCK
-        column = lax.broadcasted_iota(jnp.int32, (2 * HEADS, wide), 1)
+        column = lax.broadcasted_iota(jnp.int32, (pair, wide), 1)
+        for copy in cache_copies(values_hbm, vbuf, vsem, g, n):
+            copy.wait()
         for i in range(GROUP):
-            at = g * GROUP + i
-            s = order[at]
-            rows = queries[pl.ds(pl.multiple_of(s * HEADS, HEADS), HEADS), :]
-            both = jnp.concatenate([jnp.where(low, rows, 0.0), jnp.where(low, 0.0, rows)], axis=0)
-            own = jnp.sum(both * own_key[pl.ds(s, 1), :], axis=-1, keepdims=True)
-            scores = lax.dot_general(
-                both.astype(jnp.bfloat16),
-                kbuf[at, :wide, :],
-                (((1,), (1,)), ((), ())),
-                preferred_element_type=jnp.float32,
-            )
-            scores = jnp.where(column < lengths[s], scores, -jnp.inf)
+            s = order[g * GROUP + i]
+            rows = slice(i * pair, (i + 1) * pair)
+            own = jnp.sum(own_scores[g, rows, :], axis=-1, keepdims=True)
+            scores = jnp.where(column < lengths[s], scores_at[g, rows, :wide], -jnp.inf)
             highest = jnp.maximum(jnp.max(scores, axis=-1, keepdims=True), own)
             weights = jnp.exp(scores - highest)
             own_weights = jnp.exp(own - highest)
@@ -252,21 +286,14 @@
             own_contrast = (own_weights[:HEADS] * first - own_weights[HEADS:] * second).astype(
                 jnp.bfloat16
             )
-            out = jnp.dot(contrast, vbuf[at, :wide, :], preferred_element_type=jnp.float32)
+            out = jnp.dot(
+                contrast, vbuf[g * GROUP + i, :wide, :], preferred_element_type=jnp.float32
+            )
             out = out + own_contrast.astype(jnp.float32) * own_value[pl.ds(s, 1), :]
             mixed[pl.ds(pl.multiple_of(s * HEADS, HEADS), HEADS), :] = out
 
-    def run_group(g, carry):
-        need = blocks_of(order[g * GROUP + GROUP - 1])
-        for n in range(1, blocks + 1):
-
-            @pl.when(need == n)
-            def _():
-                attend_group(g, n)
-
-        return carry
-
-    lax.fori_loop(0, groups, run_group, 0)
+    by_blocks(score_group)
+    by_blocks(mix_group)
 
     pieces = []
     for h in range(HEADS):
@@ -354,6 +381,8 @@
             pltpu.VMEM((count, 2 * DK), f32),
             pltpu.VMEM((count, DV), f32),
             pltpu.VMEM((count * HEADS, DV), f32),
+            pltpu.VMEM((count // GROUP, GROUP * 2 * HEADS, 2 * DK), f32),
+            pltpu.VMEM((count // GROUP, GROUP * 2 * HEADS, keys.shape[1]), f32),
             pltpu.VMEM((slots, 2 * count), bf16),
             pltpu.SMEM((count + 1,), jnp.int32),
             pltpu.SemaphoreType.DMA((8,)),

time: 77 us -> 69.7 us (0.905)
  Pallas kernels: 21.9 us -> 15 us
    pallas_call x1, Pallas kernels: 19 us -> 12.1 us  [front(): pl.pallas_call(front_kernel, out_shape=(jax.ShapeDtypeStruct((experts, RO...]
  transfers between devices with their start and end apart: 3 -> 3, of which waited for: 0 -> 0; matrix products, arithmetic and copies ran while one was open for 0% -> 0% of each run, Pallas kernels for 25% -> 17%
where the time goes in v2:
time: 69.7 us; the launch traced here: 69.6 us
  blocking collectives  53.2 us (76%)
  Pallas kernels  15 us (22%)
    all_to_all x1, blocking collectives, per_device(): lax.all_to_all(packed, 'ep', 0, 0, axis_index_groups=lanes, tiled=True)  30.6 us
    all_to_all x1, blocking collectives, per_device(): lax.all_to_all(result, 'ep', 0, 0, axis_index_groups=lanes, tiled=True)  22.5 us
    pallas_call x1, Pallas kernels, front(): pl.pallas_call(front_kernel, out_shape=(jax.ShapeDtypeStruct((experts, RO...  12.1 us
    pallas_call x1, Pallas kernels, expert(): pl.pallas_call(expert_kernel, out_shape=jax.ShapeDtypeStruct(rows.shape,...  1.96 us
  transfers between devices with their start and end apart: 3, of which 0 were waited for; matrix products, arithmetic and copies ran while one was open for 0% of the time, Pallas kernels for 17%

profile of v2, /device:TPU:0, one launch (start us, length us, event | category | flops | bytes accessed | tf_op | source)
XLA Modules:
  0.0 69.6 jit_solution(14562397292965046733)
XLA Ops:
  0.6 0.1 collective-permute-start
  0.7 0.5 collective-permute-start.1
  1.2 0.1 collective-permute-start.2
  1.3 0.0 copy-start
  1.3 0.0 copy-start.1
  1.3 0.0 copy-start.2
  1.3 12.1 %front.1 = (bf16[64,8,1024]{2,1,0:T(8,128)(2,1)S(1)}, bf16[32,2048]{1,0:T(8,128)(2,1)S(1)}, bf16[32,128]{1,0:T(8,128)(2,1)}, bf16[32,128]{1,0:T(8,128)(2,1)}, bf16[128,512]{1,0:T(8,128)(2,1)S(1)}) custom-call(s32[32]{0:T(128)} %lengths_hbm.1, f32[8]{0:T(128)} %mixing_hbm.1, bf16[32,2048]{1,0:T(8,128)(2,1)} %hidden_hbm.1, f32[1,2048]{1,0:T(1,128)} %bitcast.14, ...), custom_call_target="tpu_custom_call" | custom-call | flops 20000000000 | bytes 26214400 | tf_op jit(solution)/shard_map/front/pallas_call | solution.py:354
  13.4 30.6 %all_to_all.10.rows = bf16[64,8,1024]{2,1,0:T(8,128)(2,1)S(1)} all-to-all(bf16[64,8,1024]{2,1,0:T(8,128)(2,1)S(1)} %get-tuple-element.8), channel_id=1, replica_groups={{0,2,4,6,8,10,12,14,16,18,20,22,24,26,28,30,32,34,36,38,40,42,44,46,48,..., dimensions={0} | all-to-all | bytes 2097152 | tf_op jit(solution)/shard_map/all_to_all | solution.py:515
  44.1 0.0 collective-permute-done.gate_b
  44.1 0.0 collective-permute-done.1.up_b
  44.1 0.0 collective-permute-done.2.down_b
  44.1 0.0 copy-done
  44.1 0.0 copy-done.1
  44.1 0.0 copy-done.2
  44.1 2.0 %expert.1 = bf16[64,8,1024]{2,1,0:T(8,128)(2,1)S(1)} custom-call(bf16[64,8,1024]{2,1,0:T(8,128)(2,1)S(1)} %all_to_all.10.rows, bf16[2048,256]{1,0:T(8,128)(2,1)S(1)} %bitcast.9, bf16[2048,256]{1,0:T(8,128)(2,1)S(1)} %collective-permute-done.gate_b, bf16[2048,256]{1,0:T(8,128)(2,1)S(1)} %bitcast.11, bf16[2048,256]{1,0:T(8,128)(2,1)S(1)} %collective-permute-done.1.up_b, ...), custom_call_target="tpu_custom_call" | custom-call | flops 3000000000 | bytes 8388608 | tf_op jit(solution)/shard_map/expert/pallas_call | solution.py:443
  46.1 22.5 %all_to_all.11.returned = bf16[64,8,1024]{2,1,0:T(8,128)(2,1)S(1)} all-to-all(bf16[64,8,1024]{2,1,0:T(8,128)(2,1)S(1)} %expert.1), channel_id=1, replica_groups={{0,2,4,6,8,10,12,14,16,18,20,22,24,26,28,30,32,34,36,38,40,42,44,46,48,..., dimensions={0} | all-to-all | bytes 2097152 | tf_op jit(solution)/shard_map/all_to_all | solution.py:519
  68.6 1.0 %combine.1 = bf16[32,2048]{1,0:T(8,128)(2,1)} custom-call(bf16[64,8,1024]{2,1,0:T(8,128)(2,1)S(1)} %all_to_all.11.returned, bf16[32,2048]{1,0:T(8,128)(2,1)S(1)} %get-tuple-element.9.residual, bf16[128,512]{1,0:T(8,128)(2,1)S(1)} %get-tuple-element.10.weighting), custom_call_target="tpu_custom_call" | custom-call | tf_op jit(solution)/shard_map/combine/pallas_call | solution.py:465
Async XLA Ops:
  0.6 43.4 %collective-permute-start = (bf16[2048,256]{1,0:T(8,128)(2,1)}, bf16[2048,256]{1,0:T(8,128)(2,1)S(1)}, u32[]{:S(2)}, u32[]{:S(2)}) collective-permute-start(bf16[2048,256]{1,0:T(8,128)(2,1)} %bitcast.8), channel_id=1, source_target_pairs={{0,1},{1,0},{2,3},{3,2},{4,5},{5,4},{6,7},{7,6},{8,9},{9,8},{10,11... | collective-permute-start | bytes 3145736 | tf_op jit(solution)/shard_map/ppermute | solution.py:496
  0.7 43.4 %collective-permute-start.1 = (bf16[2048,256]{1,0:T(8,128)(2,1)}, bf16[2048,256]{1,0:T(8,128)(2,1)S(1)}, u32[]{:S(2)}, u32[]{:S(2)}) collective-permute-start(bf16[2048,256]{1,0:T(8,128)(2,1)} %bitcast.10), channel_id=1, source_target_pairs={{0,1},{1,0},{2,3},{3,2},{4,5},{5,4},{6,7},{7,6},{8,9},{9,8},{10,11... | collective-permute-start | bytes 3145736 | tf_op jit(solution)/shard_map/ppermute | solution.py:496
  1.2 42.9 %collective-permute-start.2 = (bf16[256,2048]{1,0:T(8,128)(2,1)}, bf16[256,2048]{1,0:T(8,128)(2,1)S(1)}, u32[]{:S(2)}, u32[]{:S(2)}) collective-permute-start(bf16[256,2048]{1,0:T(8,128)(2,1)} %bitcast.12), channel_id=1, source_target_pairs={{0,1},{1,0},{2,3},{3,2},{4,5},{5,4},{6,7},{7,6},{8,9},{9,8},{10,11... | collective-permute-start | bytes 3145736 | tf_op jit(solution)/shard_map/ppermute | solution.py:496
  1.3 42.8 %copy-start = (bf16[1,2048,256]{2,1,0:T(8,128)(2,1)S(1)}, bf16[1,2048,256]{2,1,0:T(8,128)(2,1)}, u32[]{:S(2)}) copy-start(bf16[1,2048,256]{2,1,0:T(8,128)(2,1)} %param.31) | copy-start | bytes 3145732
  1.3 42.8 %copy-start.1 = (bf16[1,2048,256]{2,1,0:T(8,128)(2,1)S(1)}, bf16[1,2048,256]{2,1,0:T(8,128)(2,1)}, u32[]{:S(2)}) copy-start(bf16[1,2048,256]{2,1,0:T(8,128)(2,1)} %param.32) | copy-start | bytes 3145732
  1.3 42.8 %copy-start.2 = (bf16[1,256,2048]{2,1,0:T(8,128)(2,1)S(1)}, bf16[1,256,2048]{2,1,0:T(8,128)(2,1)}, u32[]{:S(2)}) copy-start(bf16[1,256,2048]{2,1,0:T(8,128)(2,1)} %param.33) | copy-start | bytes 3145732

commit v3 on v2

--- a/solution.py
+++ b/solution.py
@@ -15,7 +15,7 @@
 CAP = 4
 ROWS = 8
 BLOCK = 256
-GROUP = 8
+GROUP = 16
 WCHUNKS = 4
 
 epsilon = 1e-06

time: 69.7 us -> 68.9 us (0.989)
  Pallas kernels: 15 us -> 13.7 us
    pallas_call x1, Pallas kernels: 12.1 us -> 10.7 us  [front(): pl.pallas_call(front_kernel, out_shape=(jax.ShapeDtypeStruct((experts, RO...]
  transfers between devices with their start and end apart: 3 -> 3, of which waited for: 0 -> 0; matrix products, arithmetic and copies ran while one was open for 0% -> 0% of each run, Pallas kernels for 17% -> 16%
where the time goes in v3:
time: 68.9 us; the launch traced here: 68.3 us
  blocking collectives  53.2 us (77%)
  Pallas kernels  13.7 us (20%)
  between operations  0.69 us (1%)
    all_to_all x1, blocking collectives, per_device(): lax.all_to_all(packed, 'ep', 0, 0, axis_index_groups=lanes, tiled=True)  30.8 us
    all_to_all x1, blocking collectives, per_device(): lax.all_to_all(result, 'ep', 0, 0, axis_index_groups=lanes, tiled=True)  22.4 us
    pallas_call x1, Pallas kernels, front(): pl.pallas_call(front_kernel, out_shape=(jax.ShapeDtypeStruct((experts, RO...  10.7 us
    pallas_call x1, Pallas kernels, expert(): pl.pallas_call(expert_kernel, out_shape=jax.ShapeDtypeStruct(rows.shape,...  1.96 us
  transfers between devices with their start and end apart: 3, of which 0 were waited for; matrix products, arithmetic and copies ran while one was open for 0% of the time, Pallas kernels for 16%

profile of v3, /device:TPU:0, one launch (start us, length us, event | category | flops | bytes accessed | tf_op | source)
XLA Modules:
  0.0 68.3 jit_solution(3506897545349283491)
XLA Ops:
  0.6 0.1 collective-permute-start
  0.7 0.5 collective-permute-start.1
  1.2 0.1 collective-permute-start.2
  1.3 0.0 copy-start
  1.3 0.0 copy-start.1
  1.3 0.0 copy-start.2
  1.3 10.7 %front.1 = (bf16[64,8,1024]{2,1,0:T(8,128)(2,1)S(1)}, bf16[32,2048]{1,0:T(8,128)(2,1)S(1)}, bf16[32,128]{1,0:T(8,128)(2,1)}, bf16[32,128]{1,0:T(8,128)(2,1)}, bf16[128,512]{1,0:T(8,128)(2,1)S(1)}) custom-call(s32[32]{0:T(128)} %lengths_hbm.1, f32[8]{0:T(128)} %mixing_hbm.1, bf16[32,2048]{1,0:T(8,128)(2,1)} %hidden_hbm.1, f32[1,2048]{1,0:T(1,128)} %bitcast.14, ...), custom_call_target="tpu_custom_call" | custom-call | flops 20000000000 | bytes 26214400 | tf_op jit(solution)/shard_map/front/pallas_call | solution.py:354
  12.1 30.8 %all_to_all.10.rows = bf16[64,8,1024]{2,1,0:T(8,128)(2,1)S(1)} all-to-all(bf16[64,8,1024]{2,1,0:T(8,128)(2,1)S(1)} %get-tuple-element.8), channel_id=1, replica_groups={{0,2,4,6,8,10,12,14,16,18,20,22,24,26,28,30,32,34,36,38,40,42,44,46,48,..., dimensions={0} | all-to-all | bytes 2097152 | tf_op jit(solution)/shard_map/all_to_all | solution.py:515
  42.9 0.0 collective-permute-done.gate_b
  42.9 0.0 collective-permute-done.1.up_b
  42.9 0.0 collective-permute-done.2.down_b
  42.9 0.0 copy-done
  42.9 0.0 copy-done.1
  42.9 0.0 copy-done.2
  42.9 2.0 %expert.1 = bf16[64,8,1024]{2,1,0:T(8,128)(2,1)S(1)} custom-call(bf16[64,8,1024]{2,1,0:T(8,128)(2,1)S(1)} %all_to_all.10.rows, bf16[2048,256]{1,0:T(8,128)(2,1)S(1)} %bitcast.9, bf16[2048,256]{1,0:T(8,128)(2,1)S(1)} %collective-permute-done.gate_b, bf16[2048,256]{1,0:T(8,128)(2,1)S(1)} %bitcast.11, bf16[2048,256]{1,0:T(8,128)(2,1)S(1)} %collective-permute-done.1.up_b, ...), custom_call_target="tpu_custom_call" | custom-call | flops 3000000000 | bytes 8388608 | tf_op jit(solution)/shard_map/expert/pallas_call | solution.py:443
  44.9 22.4 %all_to_all.11.returned = bf16[64,8,1024]{2,1,0:T(8,128)(2,1)S(1)} all-to-all(bf16[64,8,1024]{2,1,0:T(8,128)(2,1)S(1)} %expert.1), channel_id=1, replica_groups={{0,2,4,6,8,10,12,14,16,18,20,22,24,26,28,30,32,34,36,38,40,42,44,46,48,..., dimensions={0} | all-to-all | bytes 2097152 | tf_op jit(solution)/shard_map/all_to_all | solution.py:519
  67.3 1.0 %combine.1 = bf16[32,2048]{1,0:T(8,128)(2,1)} custom-call(bf16[64,8,1024]{2,1,0:T(8,128)(2,1)S(1)} %all_to_all.11.returned, bf16[32,2048]{1,0:T(8,128)(2,1)S(1)} %get-tuple-element.9.residual, bf16[128,512]{1,0:T(8,128)(2,1)S(1)} %get-tuple-element.10.weighting), custom_call_target="tpu_custom_call" | custom-call | tf_op jit(solution)/shard_map/combine/pallas_call | solution.py:465
Async XLA Ops:
  0.6 42.2 %collective-permute-start = (bf16[2048,256]{1,0:T(8,128)(2,1)}, bf16[2048,256]{1,0:T(8,128)(2,1)S(1)}, u32[]{:S(2)}, u32[]{:S(2)}) collective-permute-start(bf16[2048,256]{1,0:T(8,128)(2,1)} %bitcast.8), channel_id=1, source_target_pairs={{0,1},{1,0},{2,3},{3,2},{4,5},{5,4},{6,7},{7,6},{8,9},{9,8},{10,11... | collective-permute-start | bytes 3145736 | tf_op jit(solution)/shard_map/ppermute | solution.py:496
  0.7 42.1 %collective-permute-start.1 = (bf16[2048,256]{1,0:T(8,128)(2,1)}, bf16[2048,256]{1,0:T(8,128)(2,1)S(1)}, u32[]{:S(2)}, u32[]{:S(2)}) collective-permute-start(bf16[2048,256]{1,0:T(8,128)(2,1)} %bitcast.10), channel_id=1, source_target_pairs={{0,1},{1,0},{2,3},{3,2},{4,5},{5,4},{6,7},{7,6},{8,9},{9,8},{10,11... | collective-permute-start | bytes 3145736 | tf_op jit(solution)/shard_map/ppermute | solution.py:496
  1.2 41.7 %collective-permute-start.2 = (bf16[256,2048]{1,0:T(8,128)(2,1)}, bf16[256,2048]{1,0:T(8,128)(2,1)S(1)}, u32[]{:S(2)}, u32[]{:S(2)}) collective-permute-start(bf16[256,2048]{1,0:T(8,128)(2,1)} %bitcast.12), channel_id=1, source_target_pairs={{0,1},{1,0},{2,3},{3,2},{4,5},{5,4},{6,7},{7,6},{8,9},{9,8},{10,11... | collective-permute-start | bytes 3145736 | tf_op jit(solution)/shard_map/ppermute | solution.py:496
  1.3 41.6 %copy-start = (bf16[1,2048,256]{2,1,0:T(8,128)(2,1)S(1)}, bf16[1,2048,256]{2,1,0:T(8,128)(2,1)}, u32[]{:S(2)}) copy-start(bf16[1,2048,256]{2,1,0:T(8,128)(2,1)} %param.31) | copy-start | bytes 3145732
  1.3 41.6 %copy-start.1 = (bf16[1,2048,256]{2,1,0:T(8,128)(2,1)S(1)}, bf16[1,2048,256]{2,1,0:T(8,128)(2,1)}, u32[]{:S(2)}) copy-start(bf16[1,2048,256]{2,1,0:T(8,128)(2,1)} %param.32) | copy-start | bytes 3145732
  1.3 41.6 %copy-start.2 = (bf16[1,256,2048]{2,1,0:T(8,128)(2,1)S(1)}, bf16[1,256,2048]{2,1,0:T(8,128)(2,1)}, u32[]{:S(2)}) copy-start(bf16[1,256,2048]{2,1,0:T(8,128)(2,1)} %param.33) | copy-start | bytes 3145732
